TPU v7x, 32 devices: a whole 2x2x4 slice. The times are simulated.
32 devices in a mesh: sp: 16 (over z, y, x), tp: 2 (over core).
Axes of the slice: x: 2, y: 2, z: 4, core: 2. Of those that a mesh axis runs over, the one named last changes fastest.
Arguments:
- latent: bfloat16 [4096, 2048], P(('sp', 'tp')), may hold values from -6 to 6
- cond: float32 [2048], replicated, may hold values from -6 to 6
- ctx_mod: float32 [2048], replicated, may hold values from -6 to 6
- context: bfloat16 [512, 2048], P(('sp', 'tp')), may hold values from -6 to 6
- shift_w: float32 [2048, 2048], P('sp', 'tp'), may hold values from -0.125 to 0.125
- scale_w: float32 [2048, 2048], P('sp', 'tp'), may hold values from -0.125 to 0.125
- gate_w: float32 [2048, 2048], P('sp', 'tp'), may hold values from -0.125 to 0.125
- norm_gain: float32 [2048], replicated, may hold values from 0.1 to 1.9
- w_qn: bfloat16 [2048, 2048], P(None, 'tp'), may hold values from -0.125 to 0.125
- w_qr: bfloat16 [2048, 1024], P(None, 'tp'), may hold values from -0.13258252 to 0.13258252
- w_kv_down: bfloat16 [2048, 512], replicated, may hold values from -0.125 to 0.125
- w_rope_key: bfloat16 [2048, 64], replicated, may hold values from -0.13258252 to 0.13258252
- kv_gain: float32 [512], replicated, may hold values from 0.1 to 1.9
- w_key_up: bfloat16 [512, 2048], P(None, 'tp'), may hold values from -0.66015625 to 0.66015625
- w_value_up: bfloat16 [512, 2048], P(None, 'tp'), may hold values from -0.25 to 0.25
- ctx_bias: float32 [16], P('tp'), may hold values from 2 to 3.5
- w_out: bfloat16 [2048, 2048], P('tp'), may hold values from -0.52734375 to 0.52734375
Outputs:
- mixed: bfloat16 [4096, 2048], P(('sp', 'tp'))
All inputs are finite; a program needn't handle non-finite values.
Results may differ from a plain program's by a relative error of at most 0.018.
Values may be sent and summed in bfloat16 or wider, within the bound.
A program may use at most 128 MiB of HBM per device.

v0:
```python
import jax
import jax.numpy as jnp
from jax import lax
from jax.sharding import PartitionSpec as P

GRID_W = 128
EPS = 1e-06
ROPE_BASE = 10000.0


def modulate(rows_in, gain, shift, scale):
    values = rows_in.astype(jnp.float32)
    normed = values * lax.rsqrt(jnp.mean(values * values, axis=-1, keepdims=True) + EPS)
    return (normed * gain * (1.0 + scale) + shift).astype(jnp.bfloat16)


def compress(rows_in, w_kv_down, kv_gain):
    inner = jnp.dot(rows_in, w_kv_down, preferred_element_type=jnp.float32)
    normed = inner * lax.rsqrt(jnp.mean(inner * inner, axis=-1, keepdims=True) + EPS)
    return (normed * kv_gain).astype(jnp.bfloat16)


def angles(positions, rope_dim):
    quarter = rope_dim // 4
    inverse = ROPE_BASE ** (-jnp.arange(quarter, dtype=jnp.float32) / quarter)
    row = (positions // GRID_W).astype(jnp.float32)
    column = (positions % GRID_W).astype(jnp.float32)
    return jnp.concatenate(
        [row[:, None] * inverse[None, :], column[:, None] * inverse[None, :]], axis=-1
    )


def rotate(values, angle):
    pairs = values.reshape(values.shape[:-1] + (values.shape[-1] // 2, 2))
    first = pairs[..., 0]
    second = pairs[..., 1]
    cosine = jnp.cos(angle)
    sine = jnp.sin(angle)
    turned = jnp.stack([first * cosine - second * sine, first * sine + second * cosine], axis=-1)
    return turned.reshape(values.shape)


def body(
    latent,
    cond,
    ctx_mod,
    context,
    shift_w,
    scale_w,
    gate_w,
    norm_gain,
    w_qn,
    w_qr,
    w_kv_down,
    w_rope_key,
    kv_gain,
    w_key_up,
    w_value_up,
    ctx_bias,
    w_out,
):
    n_tp = lax.axis_size("tp")
    sp_index = lax.axis_index("sp")
    tp_index = lax.axis_index("tp")
    rows = latent.shape[0]
    ctx_rows = context.shape[0]
    width = latent.shape[1]
    tok_dev = rows * n_tp
    heads_dev = ctx_bias.shape[0]
    nope = w_key_up.shape[1] // heads_dev
    vsize = w_value_up.shape[1] // heads_dev
    rope = w_rope_key.shape[1]
    period = rows + ctx_rows
    factor = (nope + rope) ** (-0.5)
    pair = jnp.stack([jax.nn.silu(cond), jax.nn.silu(ctx_mod)])
    feat_block = shift_w.shape[0]
    pair_block = lax.dynamic_slice_in_dim(pair, sp_index * feat_block, feat_block, 1)
    partials = tuple(
        (
            jnp.dot(pair_block, weight, precision=lax.Precision.HIGHEST)
            for weight in (shift_w, scale_w, gate_w)
        )
    )
    columns = shift_w.shape[1]
    placed = tuple(
        (
            lax.dynamic_update_slice_in_dim(
                jnp.zeros((2, width), jnp.float32), part, tp_index * columns, 1
            )
            for part in partials
        )
    )
    shift, scale, gate = lax.psum((placed[0], placed[1], placed[2]), ("sp", "tp"))
    h_rows = modulate(latent, norm_gain, shift[0], scale[0])
    h_ctx = modulate(context, norm_gain, shift[1], scale[1])
    own_positions = sp_index * tok_dev + tp_index * rows + jnp.arange(rows, dtype=jnp.int32)
    own_latents = jnp.concatenate(
        [compress(h_rows, w_kv_down, kv_gain), compress(h_ctx, w_kv_down, kv_gain)], axis=0
    )
    rope_rows = rotate(
        jnp.dot(h_rows, w_rope_key, preferred_element_type=jnp.float32), angles(own_positions, rope)
    ).astype(jnp.bfloat16)
    rope_ctx = jnp.dot(h_ctx, w_rope_key, preferred_element_type=jnp.float32).astype(jnp.bfloat16)
    own_rope = jnp.concatenate([rope_rows, rope_ctx], axis=0)
    piece = lax.all_gather(h_rows, "tp", axis=0, tiled=True)
    count = piece.shape[0]
    nope_part = jnp.dot(piece, w_qn, preferred_element_type=jnp.float32).astype(jnp.bfloat16)
    places = sp_index * tok_dev + jnp.arange(count, dtype=jnp.int32)
    rope_part = jnp.dot(piece, w_qr, preferred_element_type=jnp.float32).reshape(
        count, heads_dev, rope
    )
    rope_part = rotate(rope_part, angles(places, rope)[:, None, :]).reshape(count, heads_dev * rope)
    queries = jnp.concatenate([nope_part, rope_part.astype(jnp.bfloat16)], axis=1)
    query_nope = queries[:, : heads_dev * nope].reshape(tok_dev, heads_dev, nope)
    query_rope = queries[:, heads_dev * nope :].reshape(tok_dev, heads_dev, rope)

    def fold_keys(carry, keys, values, rope_keys):
        best, total, accum = carry
        count = rope_keys.shape[0]
        keys = keys.reshape(count, heads_dev, nope)
        values = values.reshape(count, heads_dev, vsize)
        scores = jnp.einsum("qhd,khd->hqk", query_nope, keys, preferred_element_type=jnp.float32)
        scores = scores + jnp.einsum(
            "qhr,kr->hqk", query_rope, rope_keys, preferred_element_type=jnp.float32
        )
        index = jnp.arange(count, dtype=jnp.int32)
        is_ctx = (index % period >= rows).astype(jnp.float32)
        scores = scores * factor + ctx_bias[:, None, None] * is_ctx[None, None, :]
        new_best = jnp.maximum(best, jnp.max(scores, axis=-1))
        weights = jnp.exp(scores - new_best[..., None])
        total = jnp.sum(weights, axis=-1)
        accum = jnp.einsum(
            "hqk,khd->hqd", weights.astype(jnp.bfloat16), values, preferred_element_type=jnp.float32
        )
        return (new_best, total, accum)

    start_carry = (
        jnp.full((heads_dev, tok_dev), -1e30, jnp.float32),
        jnp.zeros((heads_dev, tok_dev), jnp.float32),
        jnp.zeros((heads_dev, tok_dev, vsize), jnp.float32),
    )
    pieces = (
        lax.all_gather(own_latents, ("sp", "tp"), axis=0, tiled=True),
        lax.all_gather(own_rope, ("sp", "tp"), axis=0, tiled=True),
    )
    keys = jnp.dot(pieces[0], w_key_up, preferred_element_type=jnp.float32).astype(jnp.bfloat16)
    values = jnp.dot(pieces[0], w_value_up, preferred_element_type=jnp.float32).astype(jnp.bfloat16)
    best, total, accum = fold_keys(start_carry, keys, values, pieces[1])
    attended = (accum / total[..., None]).astype(jnp.bfloat16)
    attended = jnp.transpose(attended, (1, 0, 2)).reshape(tok_dev, heads_dev * vsize)
    part = attended
    branch = lax.psum_scatter(
        jnp.dot(part, w_out, preferred_element_type=jnp.float32).astype(jnp.bfloat16),
        "tp",
        scatter_dimension=0,
        tiled=True,
    ).astype(jnp.float32)
    return (latent.astype(jnp.float32) + gate[0] * branch).astype(jnp.bfloat16)


def solution(mesh):
    placed = (
        P(("sp", "tp"), None),
        P(),
        P(),
        P(("sp", "tp"), None),
        P("sp", "tp"),
        P("sp", "tp"),
        P("sp", "tp"),
        P(),
        P(None, "tp"),
        P(None, "tp"),
        P(),
        P(),
        P(),
        P(None, "tp"),
        P(None, "tp"),
        P("tp"),
        P("tp", None),
    )
    return jax.shard_map(
        body, mesh=mesh, in_specs=placed, out_specs=P(("sp", "tp"), None), check_vma=False
    )
```

profile of v0, /device:TPU:0, one launch (start us, length us, event | category | flops | bytes accessed | tf_op | source)
XLA Modules:
  0.0 253.4 jit_solution(1283834722461088093)
XLA Ops:
  8.2 1.2 fusion.17
  9.4 1.4 convolution_dynamic-update-slice_fusion.1
  10.9 1.4 convolution_dynamic-update-slice_fusion.2
  12.3 1.4 convolution_dynamic-update-slice_fusion
  13.8 42.5 %all-reduce = (f32[2,2048]{1,0:T(2,128)S(1)}, f32[2,2048]{1,0:T(2,128)S(1)}, f32[2,2048]{1,0:T(2,128)S(1)}) all-reduce(f32[2,2048]{1,0:T(2,128)S(1)} %convolution_dynamic-update-slice_fusion, f32[2,2048]{1,0:T(2,128)S(1)} %convolution_dynamic-update-slice_fusion.1, ...), channel_id=1, replica_groups=mesh['sp'=16,'tp'=2] {'sp','tp'}, use_global_device_ids=true, to_apply=%region_3.4 | all-reduce | flops 12288 | bytes 98304 | tf_op jit(solution)/shard_map/psum | solution.py:93
  56.3 2.1 fusion.21
  58.5 2.3 multiply_reduce_fusion
  60.8 1.0 fusion.26
  61.8 2.2 multiply_reduce_fusion.1
  66.4 1.3 fusion.55
  68.3 44.1 %all-gather = bf16[32,144,64]{1,2,0:T(8,128)(2,1)S(1)} all-gather(bf16[1,144,64]{1,2,0:T(8,128)(2,1)S(1)} %maximum_bitcast_fusion), channel_id=1, replica_groups=mesh['sp'=16,'tp'=2] {'sp','tp'}, dimensions={0}, use_global_device_ids=true | all-gather | bytes 608256 | tf_op jit(solution)/shard_map/all_gather | solution.py:144
  113.0 2.5 reshape.383
  115.8 2.5 fusion.56
  120.0 3.8 %fusion.10 = bf16[32,8,8,128]{3,2,1,0:T(8,128)(2,1)S(1)} fusion(bf16[256,2048]{1,0:T(8,128)(2,1)} %all-gather.4.cloned.1.call-done, bf16[2048,1024]{1,0:T(8,128)(2,1)} %param.25), kind=kOutput, calls=%fused_computation.16 | convolution fusion | flops 1074003968 | bytes 5767168 | tf_op jit(solution)/shard_map/dot_general | solution.py:107
  123.8 12.6 %all-gather.6.cloned.1.call-done = bf16[4608,512]{1,0:T(8,128)(2,1)} async-done(((bf16[144,512]{1,0:T(8,128)(2,1)}), bf16[4608,512]{1,0:T(8,128)(2,1)}) %all-gather.6.cloned.1.call-update) | async-done | bytes 4718608 | tf_op jit(solution)/shard_map/all_gather | solution.py:143
  136.4 9.5 %convolution_convert_fusion.1 = bf16[4608,1024]{0,1:T(8,128)(2,1)} fusion(bf16[4608,512]{1,0:T(8,128)(2,1)} %all-gather.6.cloned.1.call-done, bf16[512,1024]{1,0:T(8,128)(2,1)} %param.30), kind=kOutput, calls=%fused_computation.9 | convolution fusion | flops 4836556800 | bytes 15204352 | tf_op jit(solution)/shard_map/dot_general | solution.py:146
  145.9 18.4 %fusion.23 = f32[8,256,4608]{2,1,0:T(8,128)} fusion(bf16[4608,8,128]{0,2,1:T(8,128)(2,1)} %bitcast.68, bf16[32,8,8,128]{3,2,1,0:T(8,128)(2,1)S(1)} %fusion.10), kind=kOutput, calls=%fused_computation.29 | convolution fusion | flops 2415919104 | bytes 47710208 | tf_op jit(solution)/shard_map/qhd,khd->hqk/dot_general | solution.py:122
  164.3 27.8 %fusion.54 = (f32[8,256]{1,0:T(8,128)S(1)}, f32[8,256,4608]{2,1,0:T(8,128)}) fusion(f32[8,4608]{1,0:T(8,128)S(1)} %broadcast_multiply_fusion, f32[8,256,4608]{2,1,0:T(8,128)} %fusion.23, bf16[4608,64,1]{0,1,2:T(8,128)(2,1)S(1)} %copy-done.3, bf16[256,8,64]{0,2,1:T(8,128)(2,1)S(1)} %convert_element_type.105), kind=kOutput, calls=%fused_computation.103 | convolution fusion | flops 1245706240 | bytes 76505088 | tf_op jit(solution)/shard_map/qhr,kr->hqk/dot_general | solution.py:123
  192.1 16.3 %fusion.2 = f32[8,256]{1,0:T(8,128)S(1)} fusion(f32[8,256,4608]{2,1,0:T(8,128)} %get-tuple-element.29, f32[8,256]{1,0:T(8,128)S(1)} %broadcast_maximum_fusion), kind=kLoop, calls=%fused_computation.4 | loop fusion | flops 18872320 | bytes 37765120 | tf_op jit(solution)/shard_map/reduce_sum | solution.py:131
  208.4 9.9 %convolution_convert_fusion = bf16[4608,1024]{0,1:T(8,128)(2,1)} fusion(bf16[4608,512]{1,0:T(8,128)(2,1)} %all-gather.6.cloned.1.call-done, bf16[512,1024]{1,0:T(8,128)(2,1)S(1)} %copy-done.9), kind=kOutput, calls=%fused_computation.8 | convolution fusion | flops 4836556800 | bytes 15204352 | tf_op jit(solution)/shard_map/dot_general | solution.py:147
  218.3 17.5 %fusion.14 = bf16[256,8,128]{0,2,1:T(8,128)(2,1)S(1)} fusion(bf16[4608,8,128]{0,2,1:T(8,128)(2,1)} %bitcast.67, f32[8,256,4608]{2,1,0:T(8,128)} %get-tuple-element.29, f32[8,256]{1,0:T(8,128)S(1)} %broadcast_maximum_fusion, f32[256,8]{0,1:T(8,128)S(1)} %bitcast.70), kind=kOutput, calls=%fused_computation.18 | convolution fusion | flops 2435317760 | bytes 47726592 | tf_op jit(solution)/shard_map/hqk,khd->hqd/dot_general | solution.py:132
  235.8 2.2 convolution_convert_fusion.2
  238.0 6.8 %reduce-scatter.2.cloned.1.call-done = bf16[128,2048]{1,0:T(8,128)(2,1)} async-done(((bf16[256,2048]{1,0:T(8,128)(2,1)}), bf16[128,2048]{1,0:T(8,128)(2,1)}) %reduce-scatter.2.cloned.1.call-update) | async-done | bytes 524304 | tf_op jit(solution)/shard_map/reduce_scatter | solution.py:152
  244.9 2.0 fusion.22
  (62 shorter events, 7.3 us)
Async XLA Ops:
  6.5 109.3 %copy-start = (bf16[2048,512]{1,0:T(8,128)(2,1)S(1)}, bf16[2048,512]{1,0:T(8,128)(2,1)}, u32[]{:S(2)}) copy-start(bf16[2048,512]{1,0:T(8,128)(2,1)} %param.26) | copy-start | bytes 6291460
  6.5 61.4 %copy-start.6 = (f32[2048]{0:T(1024)S(1)}, f32[2048]{0:T(1024)}, u32[]{:S(2)}) copy-start(f32[2048]{0:T(1024)} %param.24) | copy-start | bytes 24580
  6.5 61.4 %copy-start.5 = (bf16[16,2048]{1,0:T(8,128)(2,1)S(1)}, bf16[16,2048]{1,0:T(8,128)(2,1)}, u32[]{:S(2)}) copy-start(bf16[16,2048]{1,0:T(8,128)(2,1)} %param.20) | copy-start | bytes 196612
  6.5 59.8 %copy-start.4 = (bf16[2048,64]{0,1:T(8,128)(2,1)S(1)}, bf16[2048,64]{0,1:T(8,128)(2,1)}, u32[]{:S(2)}) copy-start(bf16[2048,64]{0,1:T(8,128)(2,1)} %param.28) | copy-start | bytes 786436
  6.5 109.2 %copy-start.7 = (f32[8]{0:T(128)S(1)}, f32[8]{0:T(128)}, u32[]{:S(2)}) copy-start(f32[8]{0:T(128)} %param.32) | copy-start | bytes 100
  6.5 109.3 %all-gather.4.cloned.1.call-start = ((), (), s32[]{:S(2)}) async-start(), calls=%async_computation.1 | async-start | bytes 1572864 | tf_op jit(solution)/shard_map/all_gather | solution.py:105
  58.4 78.0 %all-gather.6.cloned.1.call-start = ((), (), s32[]{:S(2)}) async-start(), calls=%async_computation.2 | async-start | bytes 4866048 | tf_op jit(solution)/shard_map/all_gather | solution.py:143
  66.2 178.6 %reduce-scatter.2.cloned.1.call-start = ((), (), s32[]{:S(2)}) async-start(), calls=%async_computation.3 | async-start | bytes 1572864 | tf_op jit(solution)/shard_map/reduce_scatter | solution.py:152
  145.9 18.4 %copy-start.3 = (bf16[4608,64,1]{0,1,2:T(8,128)(2,1)S(1)}, bf16[4608,64,1]{0,1,2:T(8,128)(2,1)}, u32[]{:S(2)}) copy-start(bf16[4608,64,1]{0,1,2:T(8,128)(2,1)} %reshape.383) | copy-start | bytes 1769476
  192.1 16.3 %copy-start.9 = (bf16[512,1024]{1,0:T(8,128)(2,1)S(1)}, bf16[512,1024]{1,0:T(8,128)(2,1)}, u32[]{:S(2)}) copy-start(bf16[512,1024]{1,0:T(8,128)(2,1)} %param.31) | copy-start | bytes 3145732
  218.2 17.5 %copy-start.8 = (bf16[1024,2048]{1,0:T(8,128)(2,1)S(1)}, bf16[1024,2048]{1,0:T(8,128)(2,1)}, u32[]{:S(2)}) copy-start(bf16[1024,2048]{1,0:T(8,128)(2,1)} %param.33) | copy-start | bytes 12582916
  218.2 26.6 %copy-start.2 = (bf16[128,2048]{1,0:T(8,128)(2,1)S(1)}, bf16[128,2048]{1,0:T(8,128)(2,1)}, u32[]{:S(2)}) copy-start(bf16[128,2048]{1,0:T(8,128)(2,1)} %param.17) | copy-start | bytes 1572868
  218.3 28.6 %copy-start.1 = (bf16[2048,512]{1,0:T(8,128)(2,1)S(1)}, bf16[2048,512]{1,0:T(8,128)(2,1)}, u32[]{:S(2)}) copy-start(bf16[2048,512]{1,0:T(8,128)(2,1)} %param.26) | copy-start | bytes 6291460
Sparse Core Ops, SparseCore 0:
  58.5 8.8 all-gather.3
  70.3 66.0 all-gather.5
  238.1 6.6 reduce-scatter.1
where the time goes:
time: 254 us; the launch traced here: 253 us
  matrix products  102 us (40%)
  blocking collectives  86.6 us (34%)
  other arithmetic  28.2 us (11%)
  waiting for transfers between devices  19.5 us (8%)
  between operations  13.4 us (5%)
  local copies, waits for them, and re-layouts  3.69 us (1%)
    all_gather x1, blocking collectives, body(): lax.all_gather(own_rope, ('sp', 'tp'), axis=0, tiled=True)  44.1 us
    psum x1, blocking collectives, body(): lax.psum((placed[0], placed[1], placed[2]), ('sp', 'tp'))  42.5 us
    dot_general x1, matrix products, fold_keys(): jnp.einsum('qhr,kr->hqk', query_rope, rope_keys, preferred_element_type=j...  27.8 us
    dot_general x1, matrix products, fold_keys(): jnp.einsum('qhd,khd->hqk', query_nope, keys, preferred_element_type=jnp.f...  18.4 us
    dot_general x1, matrix products, fold_keys(): jnp.einsum('hqk,khd->hqd', weights.astype(jnp.bfloat16), values, preferre...  17.5 us
    reduce_sum x1, other arithmetic, fold_keys(): total = jnp.sum(weights, axis=-1)  16.3 us
    all_gather x1, waiting for transfers between devices, body(): lax.all_gather(own_latents, ('sp', 'tp'), axis=0, tiled=True)  12.6 us
    dot_general x1, matrix products, body(): jnp.dot(pieces[0], w_value_up, preferred_element_type=jnp.float32)  9.87 us
  transfers between devices with their start and end apart: 3, of which 2 were waited for; matrix products, arithmetic and copies ran while one was open for 8% of the time, Pallas kernels for 0%

commit v1 on v0

--- a/solution.py
+++ b/solution.py
@@ -90,7 +90,7 @@
             for part in partials
         )
     )
-    shift, scale, gate = lax.psum((placed[0], placed[1], placed[2]), ("sp", "tp"))
+    shift, scale, gate = lax.psum(lax.psum((placed[0], placed[1], placed[2]), "tp"), "sp")
     h_rows = modulate(latent, norm_gain, shift[0], scale[0])
     h_ctx = modulate(context, norm_gain, shift[1], scale[1])
     own_positions = sp_index * tok_dev + tp_index * rows + jnp.arange(rows, dtype=jnp.int32)

time: 254 us -> 291 us (1.15)
  blocking collectives: 86.6 us -> 123 us
    psum x1 -> x2, blocking collectives: 42.5 us -> 82.2 us  [the longest x1 78.4 us: body(): lax.psum(lax.psum((placed[0], placed[1], placed[2]), 'tp'), 'sp')]
    all_gather x1, blocking collectives: 44.1 us -> 40.7 us  [body(): lax.all_gather(own_rope, ('sp', 'tp'), axis=0, tiled=True)]
  transfers between devices with their start and end apart: 3 -> 3, of which waited for: 2 -> 2; matrix products, arithmetic and copies ran while one was open for 8% -> 7% of each run, Pallas kernels for 0% -> 0%
where the time goes in v1:
time: 291 us; the launch traced here: 290 us
  blocking collectives  123 us (42%)
  matrix products  102 us (35%)
  other arithmetic  28.2 us (10%)
  waiting for transfers between devices  20.5 us (7%)
  between operations  13.4 us (5%)
  local copies, waits for them, and re-layouts  3.7 us (1%)
    psum x1, blocking collectives, body(): lax.psum(lax.psum((placed[0], placed[1], placed[2]), 'tp'), 'sp')  78.4 us
    all_gather x1, blocking collectives, body(): lax.all_gather(own_rope, ('sp', 'tp'), axis=0, tiled=True)  40.7 us
    dot_general x1, matrix products, fold_keys(): jnp.einsum('qhr,kr->hqk', query_rope, rope_keys, preferred_element_type=j...  27.7 us
    dot_general x1, matrix products, fold_keys(): jnp.einsum('qhd,khd->hqk', query_nope, keys, preferred_element_type=jnp.f...  18.4 us
    dot_general x1, matrix products, fold_keys(): jnp.einsum('hqk,khd->hqd', weights.astype(jnp.bfloat16), values, preferre...  17.5 us
    reduce_sum x1, other arithmetic, fold_keys(): total = jnp.sum(weights, axis=-1)  16.3 us
    all_gather x1, waiting for transfers between devices, body(): lax.all_gather(own_latents, ('sp', 'tp'), axis=0, tiled=True)  13.6 us
    dot_general x1, matrix products, body(): jnp.dot(pieces[0], w_value_up, preferred_element_type=jnp.float32)  9.85 us
  transfers between devices with their start and end apart: 3, of which 2 were waited for; matrix products, arithmetic and copies ran while one was open for 7% of the time, Pallas kernels for 0%

profile of v1, /device:TPU:0, one launch (start us, length us, event | category | flops | bytes accessed | tf_op | source)
XLA Modules:
  0.0 290.4 jit_solution(8415639273513257800)
XLA Ops:
  8.2 1.2 fusion.17
  9.4 1.4 convolution_dynamic-update-slice_fusion.1
  10.9 1.4 convolution_dynamic-update-slice_fusion.2
  12.3 1.4 convolution_dynamic-update-slice_fusion
  13.8 3.9 %all-reduce.1 = (f32[2,2048]{1,0:T(2,128)S(1)}, f32[2,2048]{1,0:T(2,128)S(1)}, f32[2,2048]{1,0:T(2,128)S(1)}) all-reduce(f32[2,2048]{1,0:T(2,128)S(1)} %convolution_dynamic-update-slice_fusion, f32[2,2048]{1,0:T(2,128)S(1)} %convolution_dynamic-update-slice_fusion.1, ...), channel_id=1, replica_groups=mesh['sp'=16,'tp'=2] {'tp'}, use_global_device_ids=true, to_apply=%region_5.6 | all-reduce | flops 12288 | bytes 98304 | tf_op jit(solution)/shard_map/psum | solution.py:93
  17.6 78.4 %all-reduce = (f32[2,2048]{1,0:T(2,128)S(1)}, f32[2,2048]{1,0:T(2,128)S(1)}, f32[2,2048]{1,0:T(2,128)S(1)}) all-reduce(f32[2,2048]{1,0:T(2,128)S(1)} %get-tuple-element.8, f32[2,2048]{1,0:T(2,128)S(1)} %get-tuple-element.9, f32[2,2048]{1,0:T(2,128)S(1)} %get-tuple-element.10), channel_id=1, replica_groups=mesh['sp'=16,'tp'=2] {'sp'}, use_global_device_ids=true, to_apply=%region_6.7 | all-reduce | flops 12288 | bytes 98304 | tf_op jit(solution)/shard_map/psum | solution.py:93
  96.0 2.1 fusion.21
  98.2 2.3 multiply_reduce_fusion
  101.5 2.3 multiply_reduce_fusion.1
  106.2 1.3 fusion.55
  108.1 40.7 %all-gather = bf16[32,144,64]{1,2,0:T(8,128)(2,1)S(1)} all-gather(bf16[1,144,64]{1,2,0:T(8,128)(2,1)S(1)} %maximum_bitcast_fusion), channel_id=1, replica_groups=mesh['sp'=16,'tp'=2] {'sp','tp'}, dimensions={0}, use_global_device_ids=true | all-gather | bytes 608256 | tf_op jit(solution)/shard_map/all_gather | solution.py:144
  149.4 2.5 reshape.383
  152.3 2.2 fusion.56
  156.2 3.8 %fusion.10 = bf16[32,8,8,128]{3,2,1,0:T(8,128)(2,1)S(1)} fusion(bf16[256,2048]{1,0:T(8,128)(2,1)} %all-gather.4.cloned.1.call-done, bf16[2048,1024]{1,0:T(8,128)(2,1)} %param.25), kind=kOutput, calls=%fused_computation.16 | convolution fusion | flops 1074003968 | bytes 5767168 | tf_op jit(solution)/shard_map/dot_general | solution.py:107
  159.9 13.6 %all-gather.6.cloned.1.call-done = bf16[4608,512]{1,0:T(8,128)(2,1)} async-done(((bf16[144,512]{1,0:T(8,128)(2,1)}), bf16[4608,512]{1,0:T(8,128)(2,1)}) %all-gather.6.cloned.1.call-update) | async-done | bytes 4718608 | tf_op jit(solution)/shard_map/all_gather | solution.py:143
  173.5 9.4 %convolution_convert_fusion.1 = bf16[4608,1024]{0,1:T(8,128)(2,1)} fusion(bf16[4608,512]{1,0:T(8,128)(2,1)} %all-gather.6.cloned.1.call-done, bf16[512,1024]{1,0:T(8,128)(2,1)} %param.30), kind=kOutput, calls=%fused_computation.9 | convolution fusion | flops 4836556800 | bytes 15204352 | tf_op jit(solution)/shard_map/dot_general | solution.py:146
  183.0 18.4 %fusion.23 = f32[8,256,4608]{2,1,0:T(8,128)} fusion(bf16[4608,8,128]{0,2,1:T(8,128)(2,1)} %bitcast.68, bf16[32,8,8,128]{3,2,1,0:T(8,128)(2,1)S(1)} %fusion.10), kind=kOutput, calls=%fused_computation.29 | convolution fusion | flops 2415919104 | bytes 47710208 | tf_op jit(solution)/shard_map/qhd,khd->hqk/dot_general | solution.py:122
  201.4 27.7 %fusion.54 = (f32[8,256]{1,0:T(8,128)S(1)}, f32[8,256,4608]{2,1,0:T(8,128)}) fusion(f32[8,4608]{1,0:T(8,128)S(1)} %broadcast_multiply_fusion, f32[8,256,4608]{2,1,0:T(8,128)} %fusion.23, bf16[4608,64,1]{0,1,2:T(8,128)(2,1)S(1)} %copy-done.3, bf16[256,8,64]{0,2,1:T(8,128)(2,1)S(1)} %convert_element_type.105), kind=kOutput, calls=%fused_computation.103 | convolution fusion | flops 1245706240 | bytes 76505088 | tf_op jit(solution)/shard_map/qhr,kr->hqk/dot_general | solution.py:123
  229.1 16.3 %fusion.2 = f32[8,256]{1,0:T(8,128)S(1)} fusion(f32[8,256,4608]{2,1,0:T(8,128)} %get-tuple-element.32, f32[8,256]{1,0:T(8,128)S(1)} %broadcast_maximum_fusion), kind=kLoop, calls=%fused_computation.4 | loop fusion | flops 18872320 | bytes 37765120 | tf_op jit(solution)/shard_map/reduce_sum | solution.py:131
  245.4 9.9 %convolution_convert_fusion = bf16[4608,1024]{0,1:T(8,128)(2,1)} fusion(bf16[4608,512]{1,0:T(8,128)(2,1)} %all-gather.6.cloned.1.call-done, bf16[512,1024]{1,0:T(8,128)(2,1)S(1)} %copy-done.9), kind=kOutput, calls=%fused_computation.8 | convolution fusion | flops 4836556800 | bytes 15204352 | tf_op jit(solution)/shard_map/dot_general | solution.py:147
  255.3 17.5 %fusion.14 = bf16[256,8,128]{0,2,1:T(8,128)(2,1)S(1)} fusion(bf16[4608,8,128]{0,2,1:T(8,128)(2,1)} %bitcast.67, f32[8,256,4608]{2,1,0:T(8,128)} %get-tuple-element.32, f32[8,256]{1,0:T(8,128)S(1)} %broadcast_maximum_fusion, f32[256,8]{0,1:T(8,128)S(1)} %bitcast.70), kind=kOutput, calls=%fused_computation.18 | convolution fusion | flops 2435317760 | bytes 47726592 | tf_op jit(solution)/shard_map/hqk,khd->hqd/dot_general | solution.py:132
  272.8 2.2 convolution_convert_fusion.2
  275.1 6.8 %reduce-scatter.2.cloned.1.call-done = bf16[128,2048]{1,0:T(8,128)(2,1)} async-done(((bf16[256,2048]{1,0:T(8,128)(2,1)}), bf16[128,2048]{1,0:T(8,128)(2,1)}) %reduce-scatter.2.cloned.1.call-update) | async-done | bytes 524304 | tf_op jit(solution)/shard_map/reduce_scatter | solution.py:152
  281.9 2.0 fusion.22
  (63 shorter events, 8.2 us)
Async XLA Ops:
  6.5 145.7 %copy-start = (bf16[2048,512]{1,0:T(8,128)(2,1)S(1)}, bf16[2048,512]{1,0:T(8,128)(2,1)}, u32[]{:S(2)}) copy-start(bf16[2048,512]{1,0:T(8,128)(2,1)} %param.26) | copy-start | bytes 6291460
  6.5 101.2 %copy-start.6 = (f32[2048]{0:T(1024)S(1)}, f32[2048]{0:T(1024)}, u32[]{:S(2)}) copy-start(f32[2048]{0:T(1024)} %param.24) | copy-start | bytes 24580
  6.5 101.2 %copy-start.5 = (bf16[16,2048]{1,0:T(8,128)(2,1)S(1)}, bf16[16,2048]{1,0:T(8,128)(2,1)}, u32[]{:S(2)}) copy-start(bf16[16,2048]{1,0:T(8,128)(2,1)} %param.20) | copy-start | bytes 196612
  6.5 99.7 %copy-start.4 = (bf16[2048,64]{0,1:T(8,128)(2,1)S(1)}, bf16[2048,64]{0,1:T(8,128)(2,1)}, u32[]{:S(2)}) copy-start(bf16[2048,64]{0,1:T(8,128)(2,1)} %param.28) | copy-start | bytes 786436
  6.5 145.6 %copy-start.7 = (f32[8]{0:T(128)S(1)}, f32[8]{0:T(128)}, u32[]{:S(2)}) copy-start(f32[8]{0:T(128)} %param.32) | copy-start | bytes 100
  6.5 145.7 %all-gather.4.cloned.1.call-start = ((), (), s32[]{:S(2)}) async-start(), calls=%async_computation.1 | async-start | bytes 1572864 | tf_op jit(solution)/shard_map/all_gather | solution.py:105
  98.2 75.4 %all-gather.6.cloned.1.call-start = ((), (), s32[]{:S(2)}) async-start(), calls=%async_computation.2 | async-start | bytes 4866048 | tf_op jit(solution)/shard_map/all_gather | solution.py:143
  106.0 175.9 %reduce-scatter.2.cloned.1.call-start = ((), (), s32[]{:S(2)}) async-start(), calls=%async_computation.3 | async-start | bytes 1572864 | tf_op jit(solution)/shard_map/reduce_scatter | solution.py:152
  183.0 18.4 %copy-start.3 = (bf16[4608,64,1]{0,1,2:T(8,128)(2,1)S(1)}, bf16[4608,64,1]{0,1,2:T(8,128)(2,1)}, u32[]{:S(2)}) copy-start(bf16[4608,64,1]{0,1,2:T(8,128)(2,1)} %reshape.383) | copy-start | bytes 1769476
  229.1 16.3 %copy-start.9 = (bf16[512,1024]{1,0:T(8,128)(2,1)S(1)}, bf16[512,1024]{1,0:T(8,128)(2,1)}, u32[]{:S(2)}) copy-start(bf16[512,1024]{1,0:T(8,128)(2,1)} %param.31) | copy-start | bytes 3145732
  255.3 17.5 %copy-start.8 = (bf16[1024,2048]{1,0:T(8,128)(2,1)S(1)}, bf16[1024,2048]{1,0:T(8,128)(2,1)}, u32[]{:S(2)}) copy-start(bf16[1024,2048]{1,0:T(8,128)(2,1)} %param.33) | copy-start | bytes 12582916
  255.3 26.6 %copy-start.2 = (bf16[128,2048]{1,0:T(8,128)(2,1)S(1)}, bf16[128,2048]{1,0:T(8,128)(2,1)}, u32[]{:S(2)}) copy-start(bf16[128,2048]{1,0:T(8,128)(2,1)} %param.17) | copy-start | bytes 1572868
  255.3 28.6 %copy-start.1 = (bf16[2048,512]{1,0:T(8,128)(2,1)S(1)}, bf16[2048,512]{1,0:T(8,128)(2,1)}, u32[]{:S(2)}) copy-start(bf16[2048,512]{1,0:T(8,128)(2,1)} %param.26) | copy-start | bytes 6291460
Sparse Core Ops, SparseCore 0:
  98.3 4.8 all-gather.3
  106.2 67.3 all-gather.5
  275.2 6.6 reduce-scatter.1
